TPU v7x, 32 devices: a whole 2x2x4 slice. The times are simulated.
32 devices in a mesh: kv: 8 (over z, y), tp: 4 (over x, core).
Axes of the slice: x: 2, y: 2, z: 4, core: 2. Of those that a mesh axis runs over, the one named last changes fastest.
Arguments:
- residual: bfloat16 [256, 2048], P('kv', 'tp'), may hold values from -12 to 12
- first_gain: bfloat16 [2048], P('tp'), may hold values from 0.099609375 to 1.8984375
- first_gate: bfloat16 [2048, 5632], P('tp', 'kv'), may hold values from -0.125 to 0.125
- first_lift: bfloat16 [2048, 5632], P('tp', 'kv'), may hold values from -0.125 to 0.125
- first_down: bfloat16 [5632, 2048], P('kv', 'tp'), may hold values from -0.078125 to 0.078125
- mixer_gain: bfloat16 [2048], replicated, may hold values from 0.099609375 to 1.8984375
- proj_gate: bfloat16 [2048, 2048], P(None, 'tp'), may hold values from -0.125 to 0.125
- proj_input: bfloat16 [2048, 2048], P(None, 'tp'), may hold values from -0.125 to 0.125
- proj_write: bfloat16 [2048, 1024], P(None, 'tp'), may hold values from -0.125 to 0.125
- proj_read: bfloat16 [2048, 1024], P(None, 'tp'), may hold values from -0.125 to 0.125
- proj_step: bfloat16 [2048, 32], P(None, 'tp'), may hold values from -0.125 to 0.125
- step_bias: float32 [32], P('tp'), may hold values from -5 to -2
- rate_log: float32 [32], P('tp'), may hold values from -0.7 to 2.1
- skip_gain: float32 [32], P('tp'), may hold values from 0.5 to 2
- taps_input: bfloat16 [4, 2048], P(None, 'tp'), may hold values from -3 to 3
- taps_write: bfloat16 [4, 1024], P(None, 'tp'), may hold values from -3 to 3
- taps_read: bfloat16 [4, 1024], P(None, 'tp'), may hold values from -3 to 3
- buffer_input: bfloat16 [256, 3, 2048], P('kv', None, 'tp'), may hold values from -6 to 6
- buffer_write: bfloat16 [256, 3, 1024], P('kv', None, 'tp'), may hold values from -6 to 6
- buffer_read: bfloat16 [256, 3, 1024], P('kv', None, 'tp'), may hold values from -6 to 6
- scan_state: float32 [256, 32, 64, 128], P('kv', 'tp'), may hold values from -1.5 to 1.5
- group_gain: bfloat16 [2048], P('tp'), may hold values from 0.099609375 to 1.8984375
- proj_output: bfloat16 [2048, 2048], P('tp'), may hold values from -0.125 to 0.125
- second_gain: bfloat16 [2048], P('tp'), may hold values from 0.099609375 to 1.8984375
- second_gate: bfloat16 [2048, 5632], P('tp', 'kv'), may hold values from -0.125 to 0.125
- second_lift: bfloat16 [2048, 5632], P('tp', 'kv'), may hold values from -0.125 to 0.125
- second_down: bfloat16 [5632, 2048], P('kv', 'tp'), may hold values from -0.078125 to 0.078125
Outputs:
- residual_out: bfloat16 [256, 2048], P('kv', 'tp')
- state_out: float32 [256, 32, 64, 128], P('kv', 'tp')
All inputs are finite; a program needn't handle non-finite values.
Results may differ from a plain program's by a relative error of at most 0.023.
Values may be sent and summed in bfloat16 or wider, within the bound.
A program may use at most 64 MiB of HBM per device.

v0:
```python
import jax
import jax.numpy as jnp
from jax import lax
from jax.sharding import PartitionSpec as P

D = 2048
HEAD_DIM = 64
STATE = 128


norm_eps = 1e-06


def inverse_rms(values):
    return lax.rsqrt(jnp.mean(values * values, axis=-1, keepdims=True) + norm_eps)


def half_step(residual, gain, gate_weight, lift_weight, down_weight):
    widened = residual.astype(jnp.float32)
    row_total = lax.psum(jnp.sum(widened * widened, axis=1), "tp")
    factor = lax.rsqrt(row_total / D + norm_eps)
    normed = (widened * factor[:, None] * gain.astype(jnp.float32)[None, :]).astype(jnp.bfloat16)
    hidden_cols = gate_weight.shape[1]
    row_piece = lax.all_gather(normed, "kv", axis=0, tiled=True)
    gate_part = jnp.dot(row_piece, gate_weight, preferred_element_type=jnp.float32).astype(
        jnp.bfloat16
    )
    lift_part = jnp.dot(row_piece, lift_weight, preferred_element_type=jnp.float32).astype(
        jnp.bfloat16
    )
    joined = lax.optimization_barrier(jnp.concatenate([gate_part, lift_part], axis=1))
    partial_value = joined.astype(jnp.float32)
    share = lax.psum_scatter(
        partial_value.astype(jnp.bfloat16), "tp", scatter_dimension=0, tiled=True
    ).astype(jnp.float32)
    active = (jax.nn.silu(share[:, :hidden_cols]) * share[:, hidden_cols:]).astype(jnp.bfloat16)
    hidden = lax.all_gather(active, "tp", axis=0, tiled=True)
    branch = lax.psum_scatter(
        jnp.dot(hidden, down_weight, preferred_element_type=jnp.float32).astype(jnp.bfloat16),
        "kv",
        scatter_dimension=0,
        tiled=True,
    ).astype(jnp.float32)
    return (widened + 0.5 * branch).astype(jnp.bfloat16)


def short_conv(tap_weights, buffer, newest):
    taps_f = tap_weights.astype(jnp.float32)
    summed = jnp.sum(buffer.astype(jnp.float32) * taps_f[None, :-1, :], axis=1)
    summed = summed + newest.astype(jnp.float32) * taps_f[-1][None, :]
    return jax.nn.silu(summed)


def state_mixer(
    residual,
    mixer_gain,
    proj_gate,
    proj_input,
    proj_write,
    proj_read,
    proj_step,
    step_bias,
    rate_log,
    skip_gain,
    taps_input,
    taps_write,
    taps_read,
    buffer_input,
    buffer_write,
    buffer_read,
    scan_state,
    group_gain,
    proj_output,
):
    seq_rows = residual.shape[0]
    full_rows = lax.all_gather(residual, "tp", axis=1, tiled=True)
    widened = full_rows.astype(jnp.float32)
    normed = (widened * inverse_rms(widened) * mixer_gain.astype(jnp.float32)[None, :]).astype(
        jnp.bfloat16
    )

    def state_project(weight):
        return jnp.dot(normed, weight, preferred_element_type=jnp.float32).astype(jnp.bfloat16)

    gate_z = state_project(proj_gate)
    input_new = state_project(proj_input)
    write_new = state_project(proj_write)
    read_new = state_project(proj_read)
    step_raw = state_project(proj_step)
    input_conv = short_conv(taps_input, buffer_input, input_new)
    write_conv = short_conv(taps_write, buffer_write, write_new)
    read_conv = short_conv(taps_read, buffer_read, read_new)
    head_count = proj_step.shape[1]
    group_count = proj_write.shape[1] // STATE
    per_group = head_count // group_count
    step = jax.nn.softplus(step_raw.astype(jnp.float32) + step_bias[None, :])
    retain = jnp.exp(-step * jnp.exp(rate_log)[None, :])
    input_heads = input_conv.reshape(seq_rows, group_count, per_group, HEAD_DIM)
    write_groups = write_conv.reshape(seq_rows, group_count, STATE)
    read_groups = read_conv.reshape(seq_rows, group_count, STATE)
    old_state = scan_state.reshape(seq_rows, group_count, per_group, HEAD_DIM, STATE)
    retain_g = retain.reshape(seq_rows, group_count, per_group)
    step_g = step.reshape(seq_rows, group_count, per_group)
    updated = (
        retain_g[..., None, None] * old_state
        + (step_g[..., None] * input_heads)[..., None] * write_groups[:, :, None, None, :]
    )
    head_out = jnp.einsum("bgrpn,bgn->bgrp", updated, read_groups, precision=lax.Precision.HIGHEST)
    head_out = head_out + skip_gain.reshape(group_count, per_group)[None, :, :, None] * input_heads
    head_short = lax.optimization_barrier(head_out.astype(jnp.bfloat16))
    gated = head_short.astype(jnp.float32).reshape(seq_rows, group_count, per_group * HEAD_DIM)
    gated = gated * jax.nn.silu(
        gate_z.astype(jnp.float32).reshape(seq_rows, group_count, per_group * HEAD_DIM)
    )
    gated = (
        gated
        * inverse_rms(gated)
        * group_gain.astype(jnp.float32).reshape(group_count, per_group * HEAD_DIM)[None]
    )
    gated = gated.reshape(seq_rows, head_count * HEAD_DIM).astype(jnp.bfloat16)
    partial_out = jnp.dot(gated, proj_output, preferred_element_type=jnp.float32).astype(
        jnp.bfloat16
    )
    partial_out = lax.optimization_barrier(partial_out).astype(jnp.float32)
    mixed = lax.psum_scatter(
        partial_out.astype(jnp.bfloat16), "tp", scatter_dimension=1, tiled=True
    ).astype(jnp.float32)
    mixed_rows = (residual.astype(jnp.float32) + mixed).astype(jnp.bfloat16)
    return (mixed_rows, updated.reshape(seq_rows, head_count, HEAD_DIM, STATE))


def per_device(
    residual,
    first_gain,
    first_gate,
    first_lift,
    first_down,
    mixer_gain,
    proj_gate,
    proj_input,
    proj_write,
    proj_read,
    proj_step,
    step_bias,
    rate_log,
    skip_gain,
    taps_input,
    taps_write,
    taps_read,
    buffer_input,
    buffer_write,
    buffer_read,
    scan_state,
    group_gain,
    proj_output,
    second_gain,
    second_gate,
    second_lift,
    second_down,
):
    first = half_step(residual, first_gain, first_gate, first_lift, first_down)
    mixed, state_out = state_mixer(
        first,
        mixer_gain,
        proj_gate,
        proj_input,
        proj_write,
        proj_read,
        proj_step,
        step_bias,
        rate_log,
        skip_gain,
        taps_input,
        taps_write,
        taps_read,
        buffer_input,
        buffer_write,
        buffer_read,
        scan_state,
        group_gain,
        proj_output,
    )
    residual_out = half_step(mixed, second_gain, second_gate, second_lift, second_down)
    return (residual_out, state_out)


def solution(mesh):
    placed = (
        P("kv", "tp"),
        P("tp"),
        P("tp", "kv"),
        P("tp", "kv"),
        P("kv", "tp"),
        P(),
        P(None, "tp"),
        P(None, "tp"),
        P(None, "tp"),
        P(None, "tp"),
        P(None, "tp"),
        P("tp"),
        P("tp"),
        P("tp"),
        P(None, "tp"),
        P(None, "tp"),
        P(None, "tp"),
        P("kv", None, "tp"),
        P("kv", None, "tp"),
        P("kv", None, "tp"),
        P("kv", "tp", None, None),
        P("tp"),
        P("tp", None),
        P("tp"),
        P("tp", "kv"),
        P("tp", "kv"),
        P("kv", "tp"),
    )
    return jax.shard_map(
        per_device,
        mesh=mesh,
        in_specs=placed,
        out_specs=(P("kv", "tp"), P("kv", "tp", None, None)),
        check_vma=False,
    )
```

profile of v0, /device:TPU:6, one launch (start us, length us, event | category | flops | bytes accessed | tf_op | source)
XLA Modules:
  0.0 350.8 jit_solution(14504042245031635717)
XLA Ops:
  7.3 0.0 reduce-scatter.16.cloned.1.call-start
  7.4 1.1 fusion.27
  8.4 5.9 %psum.14 = f32[32]{0:T(128)S(1)} all-reduce(f32[32]{0:T(128)S(1)} %fusion.27), channel_id=1, replica_groups=mesh['kv'=8,'tp'=4] {'tp'}, use_global_device_ids=true, to_apply=%region_1.0 | all-reduce | flops 32 | bytes 256 | tf_op jit(solution)/shard_map/psum | solution.py:20
  14.3 0.7 convert_element_type.148
  15.0 0.8 fusion.29
  15.9 31.2 %all_gather.15 = bf16[256,512]{1,0:T(8,128)(2,1)S(1)} all-gather(bf16[32,512]{1,0:T(8,128)(2,1)S(1)} %fusion.29), channel_id=1, replica_groups=mesh['kv'=8,'tp'=4] {'kv'}, dimensions={0}, use_global_device_ids=true | all-gather | bytes 294912 | tf_op jit(solution)/shard_map/all_gather | solution.py:24
  47.0 1.5 convolution_convert_fusion.3
  48.5 1.5 convolution_convert_fusion.4
  50.0 1.1 copy.47
  51.2 0.0 reduce-scatter.16.cloned.1.call-update
  51.2 0.0 reduce-scatter.10.cloned.1.call-start
  51.3 22.9 %reduce-scatter.16.cloned.1.call-done = bf16[64,1408]{1,0:T(8,128)(2,1)} async-done(((bf16[256,1408]{1,0:T(8,128)(2,1)}), bf16[64,1408]{1,0:T(8,128)(2,1)}) %reduce-scatter.16.cloned.1.call-update) | async-done | bytes 180240 | tf_op jit(solution)/shard_map/reduce_scatter | solution.py:33
  74.1 0.9 convert_element_type.152
  75.1 0.1 fusion.23
  75.2 6.4 %all_gather.16 = bf16[256,704]{1,0:T(8,128)(2,1)S(1)} all-gather(bf16[64,704]{1,0:T(8,128)(2,1)S(1)} %fusion.23), channel_id=1, replica_groups=mesh['kv'=8,'tp'=4] {'tp'}, dimensions={0}, use_global_device_ids=true | all-gather | bytes 450560 | tf_op jit(solution)/shard_map/all_gather | solution.py:37
  81.6 2.2 convolution_convert_fusion.6
  83.8 0.0 reduce-scatter.10.cloned.1.call-update
  83.8 0.0 reduce-scatter.12.cloned.1.call-start
  84.0 0.1 mul.301
  84.2 63.3 %reduce-scatter.10.cloned.1.call-done = bf16[32,512]{1,0:T(8,128)(2,1)} async-done(((bf16[256,512]{1,0:T(8,128)(2,1)}), bf16[32,512]{1,0:T(8,128)(2,1)}) %reduce-scatter.10.cloned.1.call-update) | async-done | bytes 32784 | tf_op jit(solution)/shard_map/reduce_scatter | solution.py:38
  147.5 0.8 fusion.30
  148.3 5.4 %all_gather.17 = bf16[32,2048]{1,0:T(8,128)(2,1)S(1)} all-gather(bf16[32,512]{1,0:T(8,128)(2,1)S(1)} %fusion.30), channel_id=1, replica_groups=mesh['kv'=8,'tp'=4] {'tp'}, dimensions={1}, use_global_device_ids=true | all-gather | bytes 163840 | tf_op jit(solution)/shard_map/all_gather | solution.py:76
  153.7 0.1 fusion.19
  153.8 1.6 divide_multiply_fusion.3
  155.4 1.6 divide_multiply_fusion.2
  157.0 2.1 fusion.7
  159.2 0.2 multiply_exponential_fusion
  159.4 0.1 copy.41
  159.5 0.1 copy.40
  159.6 2.1 divide_multiply_fusion.1
  161.8 0.1 reshape.73
  161.9 0.1 broadcast_multiply_fusion.1
  162.0 22.0 %fusion = f32[32,2,1,4,64]{4,2,3,1,0:T(1,128)S(1)} fusion(f32[32,2,128,1,1]{2,3,4,1,0:T(1,128)S(1)} %bitcast.38, f32[32,2,4,64,128]{4,3,2,1,0:T(8,128)} %bitcast.33, f32[32,2,128]{2,1,0:T(2,128)S(1)} %mul.292, f32[32,2,4,64]{3,2,1,0:T(4,128)S(1)} %broadcast_multiply_fusion.1, f32[32,2,4]{2,1,0:T(2,128)S(1)} %copy.40), kind=kOutput, calls=%fused_computation.1 | convolution fusion | flops 31457280 | bytes 8586240 | tf_op jit(solution)/shard_map/bgrpn,bgn->bgrp/dot_general | solution.py:108
  184.0 0.1 add_convert_fusion
  184.2 0.1 reshape.75
  184.3 0.1 reshape.76
  184.4 0.2 fusion.26
  184.6 0.1 mul.309
  184.8 1.1 convolution_convert_fusion
  185.9 0.0 reduce-scatter.12.cloned.1.call-update
  185.9 0.0 reduce-scatter.18.cloned.1.call-start
  186.0 17.9 %reduce-scatter.12.cloned.1.call-done = bf16[32,512]{1,0:T(8,128)(2,1)} async-done(((bf16[32,2048]{1,0:T(8,128)(2,1)}), bf16[32,512]{1,0:T(8,128)(2,1)}) %reduce-scatter.12.cloned.1.call-update) | async-done | bytes 32784 | tf_op jit(solution)/shard_map/reduce_scatter | solution.py:125
  203.9 0.9 fusion.31
  204.7 6.0 %psum.15 = f32[32]{0:T(128)S(1)} all-reduce(f32[32]{0:T(128)S(1)} %fusion.31), channel_id=1, replica_groups=mesh['kv'=8,'tp'=4] {'tp'}, use_global_device_ids=true, to_apply=%region_11.12 | all-reduce | flops 32 | bytes 256 | tf_op jit(solution)/shard_map/psum | solution.py:20
  210.8 0.8 fusion.33
  211.6 31.0 %all_gather.18 = bf16[256,512]{1,0:T(8,128)(2,1)S(1)} all-gather(bf16[32,512]{1,0:T(8,128)(2,1)S(1)} %fusion.33), channel_id=1, replica_groups=mesh['kv'=8,'tp'=4] {'kv'}, dimensions={0}, use_global_device_ids=true | all-gather | bytes 294912 | tf_op jit(solution)/shard_map/all_gather | solution.py:24
  242.6 1.5 convolution_convert_fusion.1
  244.1 1.5 convolution_convert_fusion.2
  245.7 1.1 copy.49
  246.8 0.0 reduce-scatter.18.cloned.1.call-update
  246.8 0.0 reduce-scatter.14.cloned.1.call-start
  246.9 0.1 copy.43
  246.9 0.1 copy.44
  247.0 0.1 reshape.77
  247.1 0.1 broadcast_multiply_fusion
  247.2 22.5 %reduce-scatter.18.cloned.1.call-done = bf16[64,1408]{1,0:T(8,128)(2,1)} async-done(((bf16[256,1408]{1,0:T(8,128)(2,1)}), bf16[64,1408]{1,0:T(8,128)(2,1)}) %reduce-scatter.18.cloned.1.call-update) | async-done | bytes 180240 | tf_op jit(solution)/shard_map/reduce_scatter | solution.py:33
  269.7 0.9 convert_element_type.189
  270.7 0.1 fusion.22
  270.8 6.4 %all_gather.19 = bf16[256,704]{1,0:T(8,128)(2,1)S(1)} all-gather(bf16[64,704]{1,0:T(8,128)(2,1)S(1)} %fusion.22), channel_id=1, replica_groups=mesh['kv'=8,'tp'=4] {'tp'}, dimensions={0}, use_global_device_ids=true | all-gather | bytes 450560 | tf_op jit(solution)/shard_map/all_gather | solution.py:37
  277.2 2.2 convolution_convert_fusion.5
  279.4 0.0 reduce-scatter.14.cloned.1.call-update
  279.5 8.5 %multiply_add_fusion = f32[32,8,64,128]{3,2,1,0:T(8,128)} fusion(f32[32,8,64,128]{3,2,1,0:T(8,128)} %param.47, f32[32,8,128]{2,1,0:T(8,128)S(1)} %bitcast.34, f32[32,8,64]{2,1,0:T(8,128)S(1)} %broadcast_multiply_fusion, f32[32,8]{1,0:T(8,128)S(1)} %copy.43), kind=kLoop, calls=%fused_computation | loop fusion | flops 6291456 | bytes 16974848 | tf_op jit(solution)/shard_map/add | solution.py:105
  288.0 54.9 %reduce-scatter.14.cloned.1.call-done = bf16[32,512]{1,0:T(8,128)(2,1)} async-done(((bf16[256,512]{1,0:T(8,128)(2,1)}), bf16[32,512]{1,0:T(8,128)(2,1)}) %reduce-scatter.14.cloned.1.call-update) | async-done | bytes 32784 | tf_op jit(solution)/shard_map/reduce_scatter | solution.py:38
  342.9 1.4 fusion.34
  (55 shorter events, 0.4 us)
Async XLA Ops:
  7.2 177.6 %copy-start = (bf16[512,2048]{1,0:T(8,128)(2,1)S(1)}, bf16[512,2048]{1,0:T(8,128)(2,1)}, u32[]{:S(2)}) copy-start(bf16[512,2048]{1,0:T(8,128)(2,1)} %param.49) | copy-start | bytes 6291460
  7.2 140.3 %copy-start.1 = (bf16[32,512]{1,0:T(8,128)(2,1)S(1)}, bf16[32,512]{1,0:T(8,128)(2,1)}, u32[]{:S(2)}) copy-start(bf16[32,512]{1,0:T(8,128)(2,1)} %param.27) | copy-start | bytes 98308
  7.2 76.7 %copy-start.7 = (bf16[4,256]{1,0:T(4,128)(2,1)S(1)}, bf16[4,256]{1,0:T(4,128)(2,1)}, u32[]{:S(2)}) copy-start(bf16[4,256]{1,0:T(4,128)(2,1)} %param.42) | copy-start | bytes 6148
  7.2 76.7 %copy-start.8 = (bf16[4,256]{1,0:T(4,128)(2,1)S(1)}, bf16[4,256]{1,0:T(4,128)(2,1)}, u32[]{:S(2)}) copy-start(bf16[4,256]{1,0:T(4,128)(2,1)} %param.43) | copy-start | bytes 6148
  7.2 76.7 %copy-start.6 = (bf16[4,512]{1,0:T(4,128)(2,1)S(1)}, bf16[4,512]{1,0:T(4,128)(2,1)}, u32[]{:S(2)}) copy-start(bf16[4,512]{1,0:T(4,128)(2,1)} %param.41) | copy-start | bytes 12292
  7.2 76.8 %copy-start.13 = (f32[8]{0:T(128)S(1)}, f32[8]{0:T(128)}, u32[]{:S(2)}) copy-start(f32[8]{0:T(128)} %param.39) | copy-start | bytes 100
  7.2 76.8 %copy-start.14 = (f32[8]{0:T(128)S(1)}, f32[8]{0:T(128)}, u32[]{:S(2)}) copy-start(f32[8]{0:T(128)} %param.40) | copy-start | bytes 100
  7.2 76.9 %copy-start.10 = (bf16[512]{0:T(512)(128)(2,1)S(1)}, bf16[512]{0:T(512)(128)(2,1)}, u32[]{:S(2)}) copy-start(bf16[512]{0:T(512)(128)(2,1)} %param.48) | copy-start | bytes 3076
  7.3 76.8 %copy-start.9 = (bf16[2048]{0:T(1024)(128)(2,1)S(1)}, bf16[2048]{0:T(1024)(128)(2,1)}, u32[]{:S(2)}) copy-start(bf16[2048]{0:T(1024)(128)(2,1)} %param.32) | copy-start | bytes 12292
  7.3 76.8 %copy-start.4 = (bf16[32,3,256]{2,0,1:T(8,128)(2,1)S(1)}, bf16[32,3,256]{2,0,1:T(8,128)(2,1)}, u32[]{:S(2)}) copy-start(bf16[32,3,256]{2,0,1:T(8,128)(2,1)} %param.46) | copy-start | bytes 147460
  7.3 76.9 %copy-start.5 = (bf16[32,3,256]{2,0,1:T(8,128)(2,1)S(1)}, bf16[32,3,256]{2,0,1:T(8,128)(2,1)}, u32[]{:S(2)}) copy-start(bf16[32,3,256]{2,0,1:T(8,128)(2,1)} %param.45) | copy-start | bytes 147460
  7.3 76.9 %copy-start.3 = (bf16[32,3,512]{2,0,1:T(8,128)(2,1)S(1)}, bf16[32,3,512]{2,0,1:T(8,128)(2,1)}, u32[]{:S(2)}) copy-start(bf16[32,3,512]{2,0,1:T(8,128)(2,1)} %param.44) | copy-start | bytes 294916
  7.3 151.8 %copy-start.15 = (f32[8]{0:T(128)S(1)}, f32[8]{0:T(128)}, u32[]{:S(2)}) copy-start(f32[8]{0:T(128)} %param.38) | copy-start | bytes 100
  7.3 151.8 %copy-start.12 = (bf16[2048,8]{0,1:T(8,128)(2,1)S(1)}, bf16[2048,8]{0,1:T(8,128)(2,1)}, u32[]{:S(2)}) copy-start(bf16[2048,8]{0,1:T(8,128)(2,1)} %param.37) | copy-start | bytes 98308
  7.3 66.8 %reduce-scatter.16.cloned.1.call-start = ((), (), s32[]{:S(2)}) async-start(), calls=%async_computation.8 | async-start | bytes 901120 | tf_op jit(solution)/shard_map/reduce_scatter | solution.py:33
  51.2 96.3 %reduce-scatter.10.cloned.1.call-start = ((), (), s32[]{:S(2)}) async-start(), calls=%async_computation.5 | async-start | bytes 294912 | tf_op jit(solution)/shard_map/reduce_scatter | solution.py:38
  83.8 120.0 %reduce-scatter.12.cloned.1.call-start = ((), (), s32[]{:S(2)}) async-start(), calls=%async_computation.6 | async-start | bytes 163840 | tf_op jit(solution)/shard_map/reduce_scatter | solution.py:125
  159.2 26.8 %copy-start.11 = (bf16[512]{0:T(512)(128)(2,1)S(1)}, bf16[512]{0:T(512)(128)(2,1)}, u32[]{:S(2)}) copy-start(bf16[512]{0:T(512)(128)(2,1)} %param.50) | copy-start | bytes 3076
  185.9 83.8 %reduce-scatter.18.cloned.1.call-start = ((), (), s32[]{:S(2)}) async-start(), calls=%async_computation.9 | async-start | bytes 901120 | tf_op jit(solution)/shard_map/reduce_scatter | solution.py:33
  246.8 96.1 %reduce-scatter.14.cloned.1.call-start = ((), (), s32[]{:S(2)}) async-start(), calls=%async_computation.7 | async-start | bytes 294912 | tf_op jit(solution)/shard_map/reduce_scatter | solution.py:38
  279.5 63.4 %copy-start.2 = (bf16[32,512]{1,0:T(8,128)(2,1)S(1)}, bf16[32,512]{1,0:T(8,128)(2,1)}, u32[]{:S(2)}) copy-start(bf16[32,512]{1,0:T(8,128)(2,1)} %reduce-scatter.12.cloned.1.call-done) | copy-start | bytes 98308
Sparse Core Ops, SparseCore 0:
  51.3 22.7 reduce-scatter.15
  83.9 63.4 reduce-scatter.9
  186.0 17.7 reduce-scatter.11
  246.9 22.7 reduce-scatter.17
  279.5 63.2 reduce-scatter.13
where the time goes:
time: 353 us; the launch traced here: 351 us
  waiting for transfers between devices  182 us (52%)
  blocking collectives  92.4 us (26%)
  matrix products  41.1 us (12%)
  other arithmetic  18 us (5%)
  between operations  14.3 us (4%)
    reduce_scatter x2, waiting for transfers between devices, half_step(): lax.psum_scatter(jnp.dot(hidden, down_weight, preferred_element_type=jnp....  118 us
    all_gather x2, blocking collectives, half_step(): row_piece = lax.all_gather(normed, 'kv', axis=0, tiled=True)  62.1 us
    reduce_scatter x2, waiting for transfers between devices, half_step(): lax.psum_scatter(partial_value.astype(jnp.bfloat16), 'tp', scatter_dimens...  45.4 us
    dot_general x1, matrix products, state_mixer(): jnp.einsum('bgrpn,bgn->bgrp', updated, read_groups, precision=lax.Precisi...  22 us
    reduce_scatter x1, waiting for transfers between devices, state_mixer(): lax.psum_scatter(partial_out.astype(jnp.bfloat16), 'tp', scatter_dimensio...  17.9 us
    all_gather x2, blocking collectives, half_step(): hidden = lax.all_gather(active, 'tp', axis=0, tiled=True)  12.9 us
    psum x2, blocking collectives, half_step(): row_total = lax.psum(jnp.sum(widened * widened, axis=1), 'tp')  11.9 us
    add x1, other arithmetic, state_mixer(): retain_g[..., None, None] * old_state  8.5 us
  transfers between devices with their start and end apart: 5, of which 5 were waited for; matrix products, arithmetic and copies ran while one was open for 3% of the time, Pallas kernels for 0%

commit v1 on v0

v1 whole, which is shorter than its diff:
```python
import functools

import jax
import jax.numpy as jnp
from jax import lax
from jax.experimental import pallas as pl
from jax.experimental.pallas import tpu as pltpu
from jax.sharding import PartitionSpec as P

HEAD_DIM = 64
STATE = 128
EPS = 1e-06
MESH = pl.DeviceIdType.MESH
F32 = jnp.float32
BF16 = jnp.bfloat16
VMEM_LIMIT = 60 * 1024 * 1024


def silu(v):
    return v / (1.0 + jnp.exp(-v))


def dot(a, b):
    return jnp.dot(a, b, preferred_element_type=F32)


def enter(nk, nt, kv, tp):
    barrier = pltpu.get_barrier_semaphore()
    for d in range(1, nk):
        pl.semaphore_signal(
            barrier, inc=1, device_id={"kv": lax.rem(kv + d, nk)}, device_id_type=MESH
        )
    for d in range(1, nt):
        pl.semaphore_signal(
            barrier, inc=1, device_id={"tp": lax.rem(tp + d, nt)}, device_id_type=MESH
        )
    pl.semaphore_wait(barrier, nk + nt - 2)


def far_first(n):
    return sorted(range(1, n), key=lambda d: -min(d, n - d))


def remote(src, dst, send, recv, where):
    return pltpu.make_async_remote_copy(
        src_ref=src, dst_ref=dst, send_sem=send, recv_sem=recv,
        device_id=where, device_id_type=MESH,
    )


def half_scratch(nk, nt, rows, width, cols):
    total = nk * rows
    share = total // nt
    dma = pltpu.SemaphoreType.DMA
    return [
        pltpu.VMEM((width, cols), BF16),
        pltpu.VMEM((width, cols), BF16),
        pltpu.VMEM((cols, width), BF16),
        dma((3,)),
        pltpu.VMEM((total, width), BF16),
        pltpu.VMEM((total, width), BF16),
        pltpu.VMEM((total, 128), F32),
        pltpu.VMEM((nt, share, 128), F32),
        pltpu.VMEM((nt, 2, share, cols), BF16),
        pltpu.VMEM((nt, 2, share, cols), BF16),
        pltpu.VMEM((total, cols), BF16),
        pltpu.VMEM((total, width), BF16),
        pltpu.VMEM((nk, rows, width), BF16),
        dma((nk,)), dma((nk,)),
        dma((nt,)), dma((nt,)),
        dma((nt,)), dma((nt,)),
        dma((nt,)), dma((nt,)),
        dma((nk,)), dma((nk,)),
    ]


def start_weights(gate_hbm, lift_hbm, down_hbm, scratch):
    wg, wu, wd, wsem = scratch[:4]
    copies = [
        pltpu.make_async_copy(gate_hbm, wg, wsem.at[0]),
        pltpu.make_async_copy(lift_hbm, wu, wsem.at[1]),
        pltpu.make_async_copy(down_hbm, wd, wsem.at[2]),
    ]
    for c in copies:
        c.start()
    return copies


def half_body(nk, nt, kv, tp, x_ref, gain_ref, weights, scratch):
    (wg, wu, wd, _, xall, xg, ssq, ssr, part, parr, hid, dpart, dparr,
     ag_s, ag_r, sq_s, sq_r, rs_s, rs_r, hg_s, hg_r, dn_s, dn_r) = scratch
    rows, width = x_ref.shape
    total = nk * rows
    share = total // nt
    per = share // rows
    features = width * nt
    sends = []
    gathers = []
    for d in far_first(nk):
        c = remote(x_ref, xall.at[pl.ds(kv * rows, rows)], ag_s.at[d], ag_r.at[d],
                   {"kv": lax.rem(kv + d, nk)})
        c.start()
        gathers.append(c)
    xall[pl.ds(kv * rows, rows), :] = x_ref[...]
    gain = gain_ref[...].astype(F32)
    for c in reversed(gathers):
        c.wait_recv()
    for k in range(nk):
        at = pl.ds(k * rows, rows)
        value = xall[at, :].astype(F32)
        ssq[at, :] = jnp.broadcast_to(
            jnp.sum(value * value, axis=1, keepdims=True), (rows, 128)
        )
        xg[at, :] = (value * gain).astype(BF16)
    squares = []
    for d in far_first(nt):
        to = lax.rem(tp + d, nt)
        c = remote(ssq.at[pl.ds(to * share, share)], ssr.at[d], sq_s.at[d], sq_r.at[d],
                   {"tp": to})
        c.start()
        squares.append(c)
    weights[0].wait()
    weights[1].wait()
    parts = []
    for d in far_first(nt) + [0]:
        to = lax.rem(tp + d, nt)
        a = xg[pl.ds(to * share, share), :]
        part[d, 0] = dot(a, wg[...]).astype(BF16)
        part[d, 1] = dot(a, wu[...]).astype(BF16)
        if d:
            c = remote(part.at[d], parr.at[d], rs_s.at[d], rs_r.at[d], {"tp": to})
            c.start()
            parts.append(c)
    mine = pl.ds(tp * share, share)
    sq = ssq[mine, :]
    for d, c in zip(far_first(nt), squares):
        c.wait_recv()
        sq = sq + ssr[d]
    factor = lax.rsqrt(sq[:, :1] / features + EPS)
    gate = part[0, 0].astype(F32)
    lift = part[0, 1].astype(F32)
    for d, c in reversed(list(zip(far_first(nt), parts))):
        c.wait_recv()
        gate = gate + parr[d, 0].astype(F32)
        lift = lift + parr[d, 1].astype(F32)
    gate = gate * factor
    lift = lift * factor
    hid[mine, :] = (silu(gate) * lift).astype(BF16)
    spread = {}
    for d in far_first(nt):
        c = remote(hid.at[mine], hid.at[mine], hg_s.at[d], hg_r.at[d],
                   {"tp": lax.rem(tp + d, nt)})
        c.start()
        spread[d] = c
    weights[2].wait()
    for d in [0] + list(reversed(far_first(nt))):
        if d:
            spread[d].wait_recv()
        source = lax.rem(tp + nt - d, nt)
        block = pl.ds(source * share, share)
        dpart[block, :] = dot(hid[block, :], wd[...]).astype(BF16)
        for j in range(per):
            to = source * per + j

            @pl.when(to != kv)
            def _():
                remote(dpart.at[pl.ds(to * rows, rows)], dparr.at[kv], dn_s.at[to],
                       dn_r.at[kv], {"kv": to}).start()

    acc = dpart[pl.ds(kv * rows, rows), :].astype(F32)
    for d in reversed(far_first(nk)):
        source = lax.rem(kv + nk - d, nk)
        pltpu.make_async_copy(dparr.at[source], dparr.at[source], dn_r.at[source]).wait()
        acc = acc + dparr[source].astype(F32)
    for d in far_first(nk):
        to = lax.rem(kv + d, nk)
        pltpu.make_async_copy(dparr.at[to], dparr.at[to], dn_s.at[to]).wait()
    for c in gathers + squares + parts + list(spread.values()):
        c.wait_send()
    return (x_ref[...].astype(F32) + 0.5 * acc).astype(BF16)


def first_kernel(nk, nt, x_ref, gain_ref, gate, lift, down, own_ref, all_ref, *scratch):
    kv, tp = lax.axis_index("kv"), lax.axis_index("tp")
    held, f_s, f_r = scratch[:3]
    scratch = scratch[3:]
    weights = start_weights(gate, lift, down, scratch)
    enter(nk, nt, kv, tp)
    out = half_body(nk, nt, kv, tp, x_ref, gain_ref, weights, scratch)
    own_ref[...] = out
    held[tp] = out
    copies = []
    for d in far_first(nt):
        c = remote(held.at[tp], held.at[tp], f_s.at[d], f_r.at[d],
                   {"tp": lax.rem(tp + d, nt)})
        c.start()
        copies.append(c)
    for c in copies:
        c.wait_recv()
    all_ref[...] = held[...]
    for c in copies:
        c.wait_send()


def second_kernel(nk, nt, own_ref, pout_ref, gain_ref, gate, lift, down, out_ref, *scratch):
    kv, tp = lax.axis_index("kv"), lax.axis_index("tp")
    arrived, x_buf, m_s, m_r = scratch[:4]
    scratch = scratch[4:]
    weights = start_weights(gate, lift, down, scratch)
    enter(nk, nt, kv, tp)
    copies = []
    for d in far_first(nt):
        to = lax.rem(tp + d, nt)
        c = remote(pout_ref.at[to], arrived.at[d], m_s.at[d], m_r.at[d], {"tp": to})
        c.start()
        copies.append(c)
    acc = own_ref[...].astype(F32) + pout_ref[tp].astype(F32)
    for d, c in zip(far_first(nt), copies):
        c.wait_recv()
        acc = acc + arrived[d].astype(F32)
    x_buf[...] = acc.astype(BF16)
    out_ref[...] = half_body(nk, nt, kv, tp, x_buf, gain_ref, weights, scratch)
    for c in copies:
        c.wait_send()


def vmem(n):
    return [pl.BlockSpec(memory_space=pltpu.VMEM)] * n


def params(cid):
    return pltpu.CompilerParams(
        collective_id=cid, has_side_effects=True, vmem_limit_bytes=VMEM_LIMIT
    )


def first_half(nk, nt, x, gain, gate, lift, down):
    rows, width = x.shape
    dma = pltpu.SemaphoreType.DMA
    return pl.pallas_call(
        functools.partial(first_kernel, nk, nt),
        out_shape=(jax.ShapeDtypeStruct(x.shape, BF16),
                   jax.ShapeDtypeStruct((nt, rows, width), BF16)),
        in_specs=vmem(2) + [pl.BlockSpec(memory_space=pl.ANY)] * 3,
        out_specs=tuple(vmem(2)),
        scratch_shapes=[pltpu.VMEM((nt, rows, width), BF16), dma((nt,)), dma((nt,))]
        + half_scratch(nk, nt, rows, width, gate.shape[1]),
        compiler_params=params(1),
        name="first_half",
    )(x, gain[None, :], gate, lift, down)


def second_half(nk, nt, own, pout, gain, gate, lift, down):
    rows, width = own.shape
    dma = pltpu.SemaphoreType.DMA
    return pl.pallas_call(
        functools.partial(second_kernel, nk, nt),
        out_shape=jax.ShapeDtypeStruct(own.shape, BF16),
        in_specs=vmem(3) + [pl.BlockSpec(memory_space=pl.ANY)] * 3,
        out_specs=vmem(1)[0],
        scratch_shapes=[pltpu.VMEM((nt, rows, width), BF16), pltpu.VMEM((rows, width), BF16),
                        dma((nt,)), dma((nt,))]
        + half_scratch(nk, nt, rows, width, gate.shape[1]),
        compiler_params=params(2),
        name="second_half",
    )(own, pout, gain[None, :], gate, lift, down)


def conv(taps_ref, buf_ref, newest):
    taps = taps_ref[...].astype(F32)
    count = taps.shape[0]
    old = buf_ref[...].astype(F32)
    acc = newest.astype(BF16).astype(F32) * taps[count - 1 : count]
    for k in range(count - 1):
        acc = acc + old[k] * taps[k : k + 1]
    return silu(acc)


def split(v):
    high = v.astype(BF16).astype(F32)
    return high, v - high


def mixer_kernel(first, gain, wz, wx, wb, wr, ws, bias, rate, skip, tx, tb, tr, bx, bb, br,
                 ggain, wo, state, pout, state_out,
                 z_s, x_s, r_s, ho_s, left_s, base_s):
    step_id = pl.program_id(0)
    nt, rows, width = first.shape
    features = nt * width
    chans = wx.shape[1]
    heads = ws.shape[1]
    groups = wb.shape[1] // STATE
    gch = chans // groups
    depth = base_s.shape[1]

    def spread(v):
        r = lax.broadcasted_iota(jnp.int32, (heads, chans), 0)
        c = lax.broadcasted_iota(jnp.int32, (heads, chans), 1)
        ind = jnp.where(c // HEAD_DIM == r, 1.0, 0.0).astype(F32)
        return jnp.dot(v, ind, precision=lax.Precision.HIGHEST, preferred_element_type=F32)

    @pl.when(step_id == 0)
    def _():
        total = jnp.zeros((rows, 1), F32)
        for t in range(nt):
            v = first[t].astype(F32)
            total = total + jnp.sum(v * v, axis=1, keepdims=True)
        factor = lax.rsqrt(total / features + EPS)
        normed = jnp.concatenate(
            [(first[t].astype(F32) * factor
              * gain[:, t * width:(t + 1) * width].astype(F32)).astype(BF16)
             for t in range(nt)], axis=1)
        z_s[...] = dot(normed, wz[...]).astype(BF16).astype(F32)
        xc = conv(tx, bx, dot(normed, wx[...]))
        x_s[...] = xc
        bc = conv(tb, bb, dot(normed, wb[...]))
        rc = conv(tr, br, dot(normed, wr[...]))
        for i in range(rows):
            r_s[i] = rc[i:i + 1]
        raw = dot(normed, ws[...]).astype(BF16).astype(F32) + bias[...]
        step = jnp.maximum(raw, 0.0) + jnp.log1p(jnp.exp(-jnp.abs(raw)))
        retain = jnp.exp(-step * jnp.exp(rate[...]))
        sx_hi, sx_lo = split(spread(step) * xc)
        re_hi, re_lo = split(spread(retain))
        pad = depth - 5 * rows
        left = jnp.concatenate(
            [sx_hi, sx_lo, sx_hi, re_hi, re_lo, jnp.zeros((pad, chans), F32)], axis=0)
        left_s[...] = left.T.astype(BF16)
        for g in range(groups):
            b_hi, b_lo = split(bc[:, g * STATE:(g + 1) * STATE])
            zero = jnp.zeros((rows, STATE), F32)
            one = jnp.ones((rows, STATE), F32)
            zpad = jnp.zeros((pad, STATE), F32)
            base_s[g, :, :STATE] = jnp.concatenate(
                [b_hi, b_hi, b_lo, zero, zero, zpad], axis=0)
            base_s[g, :, STATE:] = jnp.concatenate(
                [zero, zero, zero, one, one, zpad], axis=0)

    block = state.shape[0]
    rowmod = lax.rem(lax.broadcasted_iota(jnp.int32, (depth, 2 * STATE), 0), rows)
    pick = lax.broadcasted_iota(jnp.int32, (16, STATE), 0)
    hg = heads // groups
    for i in range(block):
        b = step_id * block + i
        for g in range(groups):
            right = jnp.where(rowmod == b, base_s[g], 0.0).astype(BF16)
            both = dot(left_s[g * gch:(g + 1) * gch, :], right)
            old = state[i, g * hg:(g + 1) * hg].reshape(gch, STATE)
            new = both[:, STATE:] * old + both[:, :STATE]
            state_out[i, g * hg:(g + 1) * hg] = new.reshape(hg, HEAD_DIM, STATE)
            r_hi, r_lo = split(r_s[b][:, g * STATE:(g + 1) * STATE])
            rr = jnp.where(pick == 0, r_hi, jnp.where(pick == 1, r_lo, 0.0)).astype(BF16)
            ho = lax.dot_general(rr, new.astype(BF16), (((1,), (1,)), ((), ())),
                                 preferred_element_type=F32)
            ho_s[b, :, g * gch:(g + 1) * gch] = jnp.sum(ho, axis=0, keepdims=True)

    @pl.when(step_id == pl.num_programs(0) - 1)
    def _():
        heads_out = jnp.concatenate([ho_s[i] for i in range(rows)], axis=0)
        out = (heads_out + spread(skip[...]) * x_s[...]).astype(BF16).astype(F32)
        gated = out * silu(z_s[...])
        pieces = []
        for g in range(groups):
            v = gated[:, g * gch:(g + 1) * gch]
            pieces.append(v * lax.rsqrt(jnp.mean(v * v, axis=1, keepdims=True) + EPS))
        gated = (jnp.concatenate(pieces, axis=1) * ggain[...].astype(F32)).astype(BF16)
        for t in range(nt):
            pout[t] = dot(gated, wo[:, t * width:(t + 1) * width]).astype(BF16)


def mixer(first, gain, wz, wx, wb, wr, ws, bias, rate, skip, tx, tb, tr, bx, bb, br,
          state, ggain, wo):
    nt, rows, width = first.shape
    chans, heads = wx.shape[1], ws.shape[1]
    groups = wb.shape[1] // STATE
    depth = -(-5 * rows // 128) * 128
    block = 4 if rows % 4 == 0 else 1
    small = [first, gain[None, :], wz, wx, wb, wr, ws, bias[None, :], rate[None, :],
             skip[None, :], tx, tb, tr] + [jnp.transpose(v, (1, 0, 2)) for v in (bx, bb, br)] + [
             ggain[None, :], wo]

    def whole(v):
        zeros = (0,) * v.ndim
        return pl.BlockSpec(v.shape, lambda i: zeros, pipeline_mode=pl.Buffered(1))

    state_spec = pl.BlockSpec((block,) + state.shape[1:], lambda i: (i, 0, 0, 0))
    return pl.pallas_call(
        mixer_kernel,
        grid=(rows // block,),
        out_shape=(jax.ShapeDtypeStruct(first.shape, BF16),
                   jax.ShapeDtypeStruct(state.shape, F32)),
        in_specs=[whole(v) for v in small] + [state_spec],
        out_specs=(pl.BlockSpec(first.shape, lambda i: (0, 0, 0)), state_spec),
        scratch_shapes=[
            pltpu.VMEM((rows, chans), F32),
            pltpu.VMEM((rows, chans), F32),
            pltpu.VMEM((rows, 1, groups * STATE), F32),
            pltpu.VMEM((rows, 1, chans), F32),
            pltpu.VMEM((chans, depth), BF16),
            pltpu.VMEM((groups, depth, 2 * STATE), F32),
        ],
        compiler_params=pltpu.CompilerParams(
            vmem_limit_bytes=VMEM_LIMIT, dimension_semantics=("arbitrary",)),
        name="mixer",
    )(*small, state)


def per_device(nk, nt, residual, first_gain, first_gate, first_lift, first_down, *rest):
    mix = rest[:18]
    second_gain, second_gate, second_lift, second_down = rest[18:]
    own, gathered = first_half(nk, nt, residual, first_gain, first_gate, first_lift, first_down)
    pout, state_out = mixer(gathered, *mix)
    out = second_half(nk, nt, own, pout, second_gain, second_gate, second_lift, second_down)
    return (out, state_out)


def solution(mesh):
    placed = (
        P("kv", "tp"),
        P("tp"),
        P("tp", "kv"),
        P("tp", "kv"),
        P("kv", "tp"),
        P(),
        P(None, "tp"),
        P(None, "tp"),
        P(None, "tp"),
        P(None, "tp"),
        P(None, "tp"),
        P("tp"),
        P("tp"),
        P("tp"),
        P(None, "tp"),
        P(None, "tp"),
        P(None, "tp"),
        P("kv", None, "tp"),
        P("kv", None, "tp"),
        P("kv", None, "tp"),
        P("kv", "tp", None, None),
        P("tp"),
        P("tp", None),
        P("tp"),
        P("tp", "kv"),
        P("tp", "kv"),
        P("kv", "tp"),
    )
    return jax.shard_map(
        functools.partial(per_device, mesh.shape["kv"], mesh.shape["tp"]),
        mesh=mesh,
        in_specs=placed,
        out_specs=(P("kv", "tp"), P("kv", "tp", None, None)),
        check_vma=False,
    )
```

time: 353 us -> 113 us (0.32)
  waiting for transfers between devices: 182 us -> 0 us
  Pallas kernels: 0 us -> 101 us
  blocking collectives: 92.4 us -> 0 us
  matrix products: 41.1 us -> 0 us
  other arithmetic: 18 us -> 0 us
  between operations: 14.3 us -> 0.69 us
  local copies, waits for them, and re-layouts: 3.4 us -> 11.7 us
    reduce_scatter x5 -> x0, waiting for transfers between devices: 181 us -> none  [the longest x2 118 us: half_step(): lax.psum_scatter(jnp.dot(hidden, down_weight, preferred_element_type=jnp....]
    pallas_call x0 -> x3, Pallas kernels: none -> 101 us  [the longest x1 40.4 us: second_half(): pl.pallas_call(functools.partial(second_kernel, nk, nt), out_shape=jax.Sh...]
    all_gather x5 -> x0, blocking collectives: 80.4 us -> none  [the longest x2 62.1 us: half_step(): row_piece = lax.all_gather(normed, 'kv', axis=0, tiled=True)]
    dot_general x13 -> x0, matrix products: 41.1 us -> none  [the longest x1 22 us: state_mixer(): jnp.einsum('bgrpn,bgn->bgrp', updated, read_groups, precision=lax.Precisi...]
    psum x2 -> x0, blocking collectives: 11.9 us -> none  [half_step(): row_total = lax.psum(jnp.sum(widened * widened, axis=1), 'tp')]
    add x1 -> x0, other arithmetic: 8.5 us -> none  [state_mixer(): retain_g[..., None, None] * old_state]
    unnamed x35 -> x20, local copies, waits for them, and re-layouts: 2.35 us -> 9.31 us
    convert_element_type x13 -> x0, other arithmetic: 6.77 us -> none  [the longest x2 2.16 us: half_step(): return (widened + 0.5 * branch).astype(jnp.bfloat16)]
  transfers between devices with their start and end apart: 5 -> 0, of which waited for: 5 -> 0; matrix products, arithmetic and copies ran while one was open for 3% -> 0% of each run, Pallas kernels for 0% -> 0%
where the time goes in v1:
time: 113 us
  Pallas kernels  101 us (89%)
  local copies, waits for them, and re-layouts  11.7 us (10%)
    pallas_call x1, Pallas kernels, second_half(): pl.pallas_call(functools.partial(second_kernel, nk, nt), out_shape=jax.Sh...  40.4 us
    pallas_call x1, Pallas kernels, first_half(): pl.pallas_call(functools.partial(first_kernel, nk, nt), out_shape=(jax.Sh...  37.1 us
    pallas_call x1, Pallas kernels, mixer(): pl.pallas_call(mixer_kernel, grid=(rows // block,), out_shape=(jax.ShapeD...  23.2 us
    unnamed x20, local copies, waits for them, and re-layouts  9.31 us

profile of v1, /device:TPU:6, one launch (start us, length us, event | category | flops | bytes accessed | tf_op | source)
XLA Modules:
  0.0 113.0 jit_solution(5885927142760900686)
XLA Ops:
  0.6 0.0 copy-start.4
  0.6 2.3 %copy.29.gate = bf16[512,704]{1,0:T(8,128)(2,1)} copy(bf16[512,704]{0,1:T(8,128)(2,1)} %param.29) | data formatting | bytes 1441792 | tf_op args[2]
  2.9 0.0 copy-start.2
  2.9 0.0 copy-start.3
  2.9 0.0 copy-start.5
  2.9 2.3 %copy.30.lift = bf16[512,704]{1,0:T(8,128)(2,1)} copy(bf16[512,704]{0,1:T(8,128)(2,1)} %param.30) | data formatting | bytes 1441792 | tf_op args[3]
  5.2 0.0 copy-done.4
  5.2 0.6 broadcast_in_dim.21.gain_ref
  5.8 37.1 %first_half.1 = (bf16[32,512]{1,0:T(8,128)(2,1)}, bf16[4,32,512]{2,1,0:T(8,128)(2,1)}) custom-call(bf16[32,512]{1,0:T(8,128)(2,1)} %x_ref.1, bf16[1,512]{1,0:T(2,128)(2,1)} %broadcast_in_dim.21.gain_ref, bf16[512,704]{1,0:T(8,128)(2,1)} %copy.29.gate, bf16[512,704]{1,0:T(8,128)(2,1)} %copy.30.lift, bf16[704,512]{1,0:T(8,128)(2,1)} %down.2), custom_call_target="tpu_custom_call" | custom-call | tf_op jit(solution)/shard_map/first_half/pallas_call | solution.py:240
  42.9 0.0 copy-done.2
  42.9 1.0 copy.31.ws
  43.9 0.0 copy-done.3
  43.9 0.6 broadcast_in_dim.22.gain
  44.5 0.0 copy-done.5
  44.5 0.6 broadcast_in_dim.26.ggain
  45.1 0.0 copy-start
  45.1 0.0 copy-start.1
  45.1 23.2 %mixer.1 = (bf16[4,32,512]{2,1,0:T(8,128)(2,1)}, f32[32,8,64,128]{3,2,1,0:T(8,128)}) custom-call(bf16[4,32,512]{2,1,0:T(8,128)(2,1)} %get-tuple-element.7.first, bf16[1,2048]{1,0:T(2,128)(2,1)} %broadcast_in_dim.22.gain, bf16[2048,512]{1,0:T(8,128)(2,1)} %wz.1, bf16[2048,512]{1,0:T(8,128)(2,1)} %wx.1, bf16[2048,256]{1,0:T(8,128)(2,1)} %wb.1, ...), custom_call_target="tpu_custom_call" | custom-call | tf_op jit(solution)/shard_map/mixer/pallas_call | solution.py:387
  68.3 0.0 copy-start.6
  68.3 0.0 copy-done
  68.3 1.2 %copy.32.gate = bf16[512,704]{1,0:T(8,128)(2,1)} copy(bf16[512,704]{0,1:T(8,128)(2,1)S(1)} %copy-done) | data formatting | bytes 1441792 | tf_op args[24]
  69.4 0.0 copy-done.1
  69.4 1.2 %copy.33.lift = bf16[512,704]{1,0:T(8,128)(2,1)} copy(bf16[512,704]{0,1:T(8,128)(2,1)S(1)} %copy-done.1) | data formatting | bytes 1441792 | tf_op args[25]
  70.6 0.0 copy-done.6
  70.6 0.6 broadcast_in_dim.27.gain_ref
  71.2 40.4 %second_half.1 = bf16[32,512]{1,0:T(8,128)(2,1)} custom-call(bf16[32,512]{1,0:T(8,128)(2,1)} %get-tuple-element.6.own_ref, bf16[4,32,512]{2,1,0:T(8,128)(2,1)} %get-tuple-element.8.pout_ref, bf16[1,512]{1,0:T(2,128)(2,1)} %broadcast_in_dim.27.gain_ref, bf16[512,704]{1,0:T(8,128)(2,1)} %copy.32.gate, bf16[512,704]{1,0:T(8,128)(2,1)} %copy.33.lift, ...), custom_call_target="tpu_custom_call" | custom-call | tf_op jit(solution)/shard_map/second_half/pallas_call | solution.py:256
  111.6 1.4 %copy.35 = bf16[32,512]{1,0:T(8,128)(2,1)} copy(bf16[32,512]{1,0:T(8,128)(2,1)} %second_half.1) | data formatting | bytes 65536
Async XLA Ops:
  0.6 4.6 %copy-start.4 = (bf16[512]{0:T(512)(128)(2,1)S(1)}, bf16[512]{0:T(512)(128)(2,1)}, u32[]{:S(2)}) copy-start(bf16[512]{0:T(512)(128)(2,1)} %param.28) | copy-start | bytes 3076
  2.9 40.0 %copy-start.2 = (bf16[2048,8]{0,1:T(8,128)(2,1)S(1)}, bf16[2048,8]{0,1:T(8,128)(2,1)}, u32[]{:S(2)}) copy-start(bf16[2048,8]{0,1:T(8,128)(2,1)} %param.37) | copy-start | bytes 98308
  2.9 41.0 %copy-start.3 = (bf16[2048]{0:T(1024)(128)(2,1)S(1)}, bf16[2048]{0:T(1024)(128)(2,1)}, u32[]{:S(2)}) copy-start(bf16[2048]{0:T(1024)(128)(2,1)} %param.32) | copy-start | bytes 12292
  2.9 41.6 %copy-start.5 = (bf16[512]{0:T(512)(128)(2,1)S(1)}, bf16[512]{0:T(512)(128)(2,1)}, u32[]{:S(2)}) copy-start(bf16[512]{0:T(512)(128)(2,1)} %param.48) | copy-start | bytes 3076
  45.1 23.2 %copy-start = (bf16[512,704]{0,1:T(8,128)(2,1)S(1)}, bf16[512,704]{0,1:T(8,128)(2,1)}, u32[]{:S(2)}) copy-start(bf16[512,704]{0,1:T(8,128)(2,1)} %param.51) | copy-start | bytes 2162692
  45.1 24.4 %copy-start.1 = (bf16[512,704]{0,1:T(8,128)(2,1)S(1)}, bf16[512,704]{0,1:T(8,128)(2,1)}, u32[]{:S(2)}) copy-start(bf16[512,704]{0,1:T(8,128)(2,1)} %param.52) | copy-start | bytes 2162692
  68.3 2.4 %copy-start.6 = (bf16[512]{0:T(512)(128)(2,1)S(1)}, bf16[512]{0:T(512)(128)(2,1)}, u32[]{:S(2)}) copy-start(bf16[512]{0:T(512)(128)(2,1)} %param.50) | copy-start | bytes 3076

commit v2 on v1

--- a/solution.py
+++ b/solution.py
@@ -22,6 +22,10 @@
 
 def dot(a, b):
     return jnp.dot(a, b, preferred_element_type=F32)
+
+
+def dot_t(a, b):
+    return lax.dot_general(a, b, (((1,), (1,)), ((), ())), preferred_element_type=F32)
 
 
 def enter(nk, nt, kv, tp):
@@ -53,8 +57,8 @@
     share = total // nt
     dma = pltpu.SemaphoreType.DMA
     return [
-        pltpu.VMEM((width, cols), BF16),
-        pltpu.VMEM((width, cols), BF16),
+        pltpu.VMEM((cols, width), BF16),
+        pltpu.VMEM((cols, width), BF16),
         pltpu.VMEM((cols, width), BF16),
         dma((3,)),
         pltpu.VMEM((total, width), BF16),
@@ -86,7 +90,7 @@
     return copies
 
 
-def half_body(nk, nt, kv, tp, x_ref, gain_ref, weights, scratch):
+def half_body(nk, nt, kv, tp, place, x_ref, gain_ref, weights, scratch):
     (wg, wu, wd, _, xall, xg, ssq, ssr, part, parr, hid, dpart, dparr,
      ag_s, ag_r, sq_s, sq_r, rs_s, rs_r, hg_s, hg_r, dn_s, dn_r) = scratch
     rows, width = x_ref.shape
@@ -102,7 +106,7 @@
         c.start()
         gathers.append(c)
     xall[pl.ds(kv * rows, rows), :] = x_ref[...]
-    gain = gain_ref[...].astype(F32)
+    gain = gain_ref[:, place * width:(place + 1) * width].astype(F32)
     for c in reversed(gathers):
         c.wait_recv()
     for k in range(nk):
@@ -125,8 +129,8 @@
     for d in far_first(nt) + [0]:
         to = lax.rem(tp + d, nt)
         a = xg[pl.ds(to * share, share), :]
-        part[d, 0] = dot(a, wg[...]).astype(BF16)
-        part[d, 1] = dot(a, wu[...]).astype(BF16)
+        part[d, 0] = dot_t(a, wg[...]).astype(BF16)
+        part[d, 1] = dot_t(a, wu[...]).astype(BF16)
         if d:
             c = remote(part.at[d], parr.at[d], rs_s.at[d], rs_r.at[d], {"tp": to})
             c.start()
@@ -186,7 +190,7 @@
     scratch = scratch[3:]
     weights = start_weights(gate, lift, down, scratch)
     enter(nk, nt, kv, tp)
-    out = half_body(nk, nt, kv, tp, x_ref, gain_ref, weights, scratch)
+    out = half_body(nk, nt, kv, tp, 0, x_ref, gain_ref, weights, scratch)
     own_ref[...] = out
     held[tp] = out
     copies = []
@@ -219,7 +223,7 @@
         c.wait_recv()
         acc = acc + arrived[d].astype(F32)
     x_buf[...] = acc.astype(BF16)
-    out_ref[...] = half_body(nk, nt, kv, tp, x_buf, gain_ref, weights, scratch)
+    out_ref[...] = half_body(nk, nt, kv, tp, 1, x_buf, gain_ref, weights, scratch)
     for c in copies:
         c.wait_send()
 
@@ -244,10 +248,10 @@
         in_specs=vmem(2) + [pl.BlockSpec(memory_space=pl.ANY)] * 3,
         out_specs=tuple(vmem(2)),
         scratch_shapes=[pltpu.VMEM((nt, rows, width), BF16), dma((nt,)), dma((nt,))]
-        + half_scratch(nk, nt, rows, width, gate.shape[1]),
+        + half_scratch(nk, nt, rows, width, gate.shape[0]),
         compiler_params=params(1),
         name="first_half",
-    )(x, gain[None, :], gate, lift, down)
+    )(x, gain, gate, lift, down)
 
 
 def second_half(nk, nt, own, pout, gain, gate, lift, down):
@@ -260,10 +264,10 @@
         out_specs=vmem(1)[0],
         scratch_shapes=[pltpu.VMEM((nt, rows, width), BF16), pltpu.VMEM((rows, width), BF16),
                         dma((nt,)), dma((nt,))]
-        + half_scratch(nk, nt, rows, width, gate.shape[1]),
+        + half_scratch(nk, nt, rows, width, gate.shape[0]),
         compiler_params=params(2),
         name="second_half",
-    )(own, pout, gain[None, :], gate, lift, down)
+    )(own, pout, gain, gate, lift, down)
 
 
 def conv(taps_ref, buf_ref, newest):
@@ -282,13 +286,13 @@
 
 
 def mixer_kernel(first, gain, wz, wx, wb, wr, ws, bias, rate, skip, tx, tb, tr, bx, bb, br,
-                 ggain, wo, state, pout, state_out,
+                 wo, state, pout, state_out,
                  z_s, x_s, r_s, ho_s, left_s, base_s):
     step_id = pl.program_id(0)
     nt, rows, width = first.shape
     features = nt * width
     chans = wx.shape[1]
-    heads = ws.shape[1]
+    heads = ws.shape[0]
     groups = wb.shape[1] // STATE
     gch = chans // groups
     depth = base_s.shape[1]
@@ -308,7 +312,7 @@
         factor = lax.rsqrt(total / features + EPS)
         normed = jnp.concatenate(
             [(first[t].astype(F32) * factor
-              * gain[:, t * width:(t + 1) * width].astype(F32)).astype(BF16)
+              * gain[:, (t + 3) * width:(t + 4) * width].astype(F32)).astype(BF16)
              for t in range(nt)], axis=1)
         z_s[...] = dot(normed, wz[...]).astype(BF16).astype(F32)
         xc = conv(tx, bx, dot(normed, wx[...]))
@@ -317,7 +321,7 @@
         rc = conv(tr, br, dot(normed, wr[...]))
         for i in range(rows):
             r_s[i] = rc[i:i + 1]
-        raw = dot(normed, ws[...]).astype(BF16).astype(F32) + bias[...]
+        raw = dot_t(normed, ws[...]).astype(BF16).astype(F32) + bias[...]
         step = jnp.maximum(raw, 0.0) + jnp.log1p(jnp.exp(-jnp.abs(raw)))
         retain = jnp.exp(-step * jnp.exp(rate[...]))
         sx_hi, sx_lo = split(spread(step) * xc)
@@ -332,9 +336,9 @@
             one = jnp.ones((rows, STATE), F32)
             zpad = jnp.zeros((pad, STATE), F32)
             base_s[g, :, :STATE] = jnp.concatenate(
-                [b_hi, b_hi, b_lo, zero, zero, zpad], axis=0)
+                [b_hi, b_hi, b_lo, zero, zero, zpad], axis=0).astype(BF16)
             base_s[g, :, STATE:] = jnp.concatenate(
-                [zero, zero, zero, one, one, zpad], axis=0)
+                [zero, zero, zero, one, one, zpad], axis=0).astype(BF16)
 
     block = state.shape[0]
     rowmod = lax.rem(lax.broadcasted_iota(jnp.int32, (depth, 2 * STATE), 0), rows)
@@ -342,8 +346,9 @@
     hg = heads // groups
     for i in range(block):
         b = step_id * block + i
+        mask = jnp.where(rowmod == b, 1.0, 0.0).astype(BF16)
         for g in range(groups):
-            right = jnp.where(rowmod == b, base_s[g], 0.0).astype(BF16)
+            right = base_s[g] * mask
             both = dot(left_s[g * gch:(g + 1) * gch, :], right)
             old = state[i, g * hg:(g + 1) * hg].reshape(gch, STATE)
             new = both[:, STATE:] * old + both[:, :STATE]
@@ -363,21 +368,21 @@
         for g in range(groups):
             v = gated[:, g * gch:(g + 1) * gch]
             pieces.append(v * lax.rsqrt(jnp.mean(v * v, axis=1, keepdims=True) + EPS))
-        gated = (jnp.concatenate(pieces, axis=1) * ggain[...].astype(F32)).astype(BF16)
+        gated = (jnp.concatenate(pieces, axis=1) * gain[:, 2 * width:3 * width].astype(F32)).astype(BF16)
         for t in range(nt):
             pout[t] = dot(gated, wo[:, t * width:(t + 1) * width]).astype(BF16)
 
 
 def mixer(first, gain, wz, wx, wb, wr, ws, bias, rate, skip, tx, tb, tr, bx, bb, br,
-          state, ggain, wo):
+          state, wo):
     nt, rows, width = first.shape
-    chans, heads = wx.shape[1], ws.shape[1]
+    chans, heads = wx.shape[1], ws.shape[0]
     groups = wb.shape[1] // STATE
     depth = -(-5 * rows // 128) * 128
     block = 4 if rows % 4 == 0 else 1
-    small = [first, gain[None, :], wz, wx, wb, wr, ws, bias[None, :], rate[None, :],
+    small = [first, gain, wz, wx, wb, wr, ws, bias[None, :], rate[None, :],
              skip[None, :], tx, tb, tr] + [jnp.transpose(v, (1, 0, 2)) for v in (bx, bb, br)] + [
-             ggain[None, :], wo]
+             wo]
 
     def whole(v):
         zeros = (0,) * v.ndim
@@ -397,7 +402,7 @@
             pltpu.VMEM((rows, 1, groups * STATE), F32),
             pltpu.VMEM((rows, 1, chans), F32),
             pltpu.VMEM((chans, depth), BF16),
-            pltpu.VMEM((groups, depth, 2 * STATE), F32),
+            pltpu.VMEM((groups, depth, 2 * STATE), BF16),
         ],
         compiler_params=pltpu.CompilerParams(
             vmem_limit_bytes=VMEM_LIMIT, dimension_semantics=("arbitrary",)),
@@ -406,11 +411,19 @@
 
 
 def per_device(nk, nt, residual, first_gain, first_gate, first_lift, first_down, *rest):
-    mix = rest[:18]
+    mix = list(rest[:18])
     second_gain, second_gate, second_lift, second_down = rest[18:]
-    own, gathered = first_half(nk, nt, residual, first_gain, first_gate, first_lift, first_down)
+    width = residual.shape[1]
+    gains = lax.optimization_barrier(
+        jnp.concatenate([first_gain, second_gain, mix[16], mix[0]])[None, :])
+    mix[0] = gains
+    del mix[16]
+    mix[5] = mix[5].T
+    own, gathered = first_half(
+        nk, nt, residual, gains, first_gate.T, first_lift.T, first_down)
     pout, state_out = mixer(gathered, *mix)
-    out = second_half(nk, nt, own, pout, second_gain, second_gate, second_lift, second_down)
+    out = second_half(nk, nt, own, pout, gains,
+                      second_gate.T, second_lift.T, second_down)
     return (out, state_out)
 
 

time: 113 us -> 104 us (0.920)
  local copies, waits for them, and re-layouts: 11.7 us -> 1.99 us
    unnamed x20 -> x1, local copies, waits for them, and re-layouts: 9.31 us -> 1.38 us
    broadcast_in_dim x4 -> x1, local copies, waits for them, and re-layouts: 2.35 us -> 0.61 us  [per_device(): jnp.concatenate([first_gain, second_gain, mix[16], mix[0]])[None, :]]
where the time goes in v2:
time: 104 us
  Pallas kernels  101 us (97%)
  local copies, waits for them, and re-layouts  1.99 us (2%)
    pallas_call x1, Pallas kernels, second_half(): pl.pallas_call(functools.partial(second_kernel, nk, nt), out_shape=jax.Sh...  40.4 us
    pallas_call x1, Pallas kernels, first_half(): pl.pallas_call(functools.partial(first_kernel, nk, nt), out_shape=(jax.Sh...  37.1 us
    pallas_call x1, Pallas kernels, mixer(): pl.pallas_call(mixer_kernel, grid=(rows // block,), out_shape=(jax.ShapeD...  23.1 us

profile of v2, /device:TPU:6, one launch (start us, length us, event | category | flops | bytes accessed | tf_op | source)
XLA Modules:
  0.0 103.9 jit_solution(14710509900785564658)
XLA Ops:
  0.6 0.7 pad_maximum_fusion
  1.4 0.6 broadcast_in_dim.12.gain_ref.gain
  2.0 37.1 %first_half.1 = (bf16[32,512]{1,0:T(8,128)(2,1)}, bf16[4,32,512]{2,1,0:T(8,128)(2,1)}) custom-call(bf16[32,512]{1,0:T(8,128)(2,1)} %x_ref.1, bf16[1,3584]{1,0:T(2,128)(2,1)} %broadcast_in_dim.12.gain_ref.gain, bf16[704,512]{1,0:T(8,128)(2,1)} %bitcast.11, bf16[704,512]{1,0:T(8,128)(2,1)} %bitcast.12, bf16[704,512]{1,0:T(8,128)(2,1)} %down.2), custom_call_target="tpu_custom_call" | custom-call | tf_op jit(solution)/shard_map/first_half/pallas_call | solution.py:244
  39.1 23.1 %mixer.1 = (bf16[4,32,512]{2,1,0:T(8,128)(2,1)}, f32[32,8,64,128]{3,2,1,0:T(8,128)}) custom-call(bf16[4,32,512]{2,1,0:T(8,128)(2,1)} %get-tuple-element.7.first, bf16[1,3584]{1,0:T(2,128)(2,1)} %broadcast_in_dim.12.gain_ref.gain, bf16[2048,512]{1,0:T(8,128)(2,1)} %wz.1, bf16[2048,512]{1,0:T(8,128)(2,1)} %wx.1, bf16[2048,256]{1,0:T(8,128)(2,1)} %wb.1, ...), custom_call_target="tpu_custom_call" | custom-call | tf_op jit(solution)/shard_map/mixer/pallas_call | solution.py:392
  62.1 40.4 %second_half.1 = bf16[32,512]{1,0:T(8,128)(2,1)} custom-call(bf16[32,512]{1,0:T(8,128)(2,1)} %get-tuple-element.6.own_ref, bf16[4,32,512]{2,1,0:T(8,128)(2,1)} %get-tuple-element.8.pout_ref, bf16[1,3584]{1,0:T(2,128)(2,1)} %broadcast_in_dim.12.gain_ref.gain, bf16[704,512]{1,0:T(8,128)(2,1)} %bitcast.13, bf16[704,512]{1,0:T(8,128)(2,1)} %bitcast.14, ...), custom_call_target="tpu_custom_call" | custom-call | tf_op jit(solution)/shard_map/second_half/pallas_call | solution.py:260
  102.6 1.4 %copy.30 = bf16[32,512]{1,0:T(8,128)(2,1)} copy(bf16[32,512]{1,0:T(8,128)(2,1)} %second_half.1) | data formatting | bytes 65536
